TPU v7x, 512 devices: a 8x2x16 block of a 8x8x16 slice. The times are simulated.
512 devices in a mesh: grp: 2 (over y), sp: 32 (over z, core), tp: 8 (over x).
Axes of the slice: x: 8, y: 2, z: 16, core: 2. Of those that a mesh axis runs over, the one named last changes fastest.
The devices are a block of a 8x8x16 slice.
Arguments:
- tokens: bfloat16 [8192, 2048], P(('grp', 'sp'), 'tp'), parts along dimension 0, may hold values from -30 to 30, as said below
- norm_gain: float32 [2, 2048], replicated, may hold values from 0.1 to 1.9
- in_weight: bfloat16 [2, 2048, 2048], P(None, 'sp', 'tp'), may hold values from -0.125 to 0.125
- gate_weight: bfloat16 [2, 2048, 2048], P(None, 'sp', 'tp'), may hold values from -0.125 to 0.125
- conv_taps: float32 [2, 4, 2048], P(None, None, 'tp'), may hold values from -3 to 3
- decay_logit: float32 [2, 2, 2048], P(None, None, 'tp'), may hold values from 4 to 20, as said below
- gate_maps: bfloat16 [2, 2048, 1024], P(None, 'tp', 'sp'), may hold values from -0.375 to 0.375
- out_weight: bfloat16 [2, 2048, 2048], P(None, 'sp', 'tp'), may hold values from -0.375 to 0.375
- final_gain: float32 [2048], P('tp'), may hold values from 0.1 to 1.9
Outputs:
- normed_out: bfloat16 [8192, 2048], P(('grp', 'sp'), 'tp'), parts along dimension 0
There are 2 independent parts, one for each index of `grp`. A program takes and returns all parts, laid end to end along the dimension named above; an argument that names none is the same for every part. Nothing has to cross between parts.
Inputs may be any that keep to these rules, and one draw needn't show every extreme that they name: Activations of order one whose scale changes by blocks of tokens and of channels. `decay_logit`: decay parameters; channels differ in how far their state reaches.
All inputs are finite; a program needn't handle non-finite values.
Results may differ from a plain program's by a relative error of at most 0.02.
Values may be sent and summed in bfloat16 or wider, within the bound.
A program may use at most 128 MiB of HBM per device.

v0:
```python
import jax
import jax.numpy as jnp
from jax import lax
from jax.sharding import PartitionSpec as P

D = 2048
HEAD_W = 256
TAPS = 4
LAYERS = 2


EPS = 1e-06


def joined_along(tiles, dim):
    tiles = jnp.moveaxis(tiles, 0, dim)
    shape = tiles.shape
    return tiles.reshape(*shape[:dim], shape[dim] * shape[dim + 1], *shape[dim + 2 :])


def gather_packed(arrays, axis, dims):
    flat = jnp.concatenate([a.reshape(-1) for a in arrays])
    lines, at, outs = (lax.all_gather(flat, axis), 0, [])
    for a, dim in zip(arrays, dims):
        tiles = lines[:, at : at + a.size].reshape(-1, *a.shape)
        outs.append(joined_along(tiles, dim))
        at += a.size
    return tuple(outs)


def from_everyone(value, axis):
    devices = lax.axis_size(axis)
    return lax.all_to_all(
        jnp.broadcast_to(value[None], (devices, *value.shape)), axis, 0, 0, tiled=True
    )


def collect(value, axis, dim):
    return joined_along(from_everyone(value, axis), dim)


def extended(value, sides, width):
    for axis, dim in sides:
        devices, length = (lax.axis_size(axis), value.shape[dim])
        up = [(i, (i + 1) % devices) for i in range(devices - 1)]
        down = [(j, i) for i, j in up]
        last = lax.slice_in_dim(value, length - width, length, axis=dim)
        leading = lax.slice_in_dim(value, 0, width, axis=dim)
        before = lax.ppermute(last, axis, up)
        after = lax.ppermute(leading, axis, down)
        value = jnp.concatenate([before, value, after], axis=dim)
    return value


def gathered_once(value, axis):
    leaves = jax.tree.leaves(value)
    sequence = sorted(range(len(leaves)), key=lambda k: -leaves[k].size)
    width = (1, *leaves[sequence[0]].shape)[-1]
    lines = [
        jnp.pad(leaves[k].reshape(-1), (0, -leaves[k].size % width)).reshape(-1, width)
        for k in sequence
    ]
    both, at, found = (from_everyone(jnp.concatenate(lines), axis), 0, {})
    for k, line in zip(sequence, lines):
        piece = both[:, at : at + len(line)].reshape(len(both), -1)
        found[k] = piece[:, : leaves[k].size].reshape(-1, *leaves[k].shape)
        at += len(line)
    numbers = iter(range(len(leaves)))
    return jax.tree.map(lambda _: found[next(numbers)], value)


def folded_in_pairs(pieces, combine):
    while len(jax.tree.leaves(pieces)[0]) > 1:
        pieces = jax.vmap(combine)(
            *(jax.tree.map(lambda part: part[side::2], pieces) for side in (0, 1))
        )
    return jax.tree.map(lambda part: part[0], pieces)


def carried_in(value, axis, combine, identity, reverse):
    devices, position = (lax.axis_size(axis), lax.axis_index(axis))
    passed = jnp.arange(devices) > position if reverse else jnp.arange(devices) < position

    def kept(part, zero, own):
        part = jnp.where(
            passed.reshape(-1, *(1 for _ in own.shape)), part, jnp.asarray(zero, own.dtype)
        )
        return part[::-1] if reverse else part

    pieces = gathered_once(value, axis)
    return folded_in_pairs(jax.tree.map(kept, pieces, identity, value), combine)


def over_copies(value, axis):
    everything = from_everyone(value, axis)
    return jnp.sum(everything, axis=0)


def combine_pair(earlier, later):
    return (earlier[0] * later[0], later[0] * earlier[1] + later[1])


def body(
    tokens,
    norm_gain,
    in_weight,
    gate_weight,
    conv_taps,
    decay_logit,
    gate_maps,
    out_weight,
    final_gain,
):
    resid = tokens
    rows = tokens.shape[0]
    width = in_weight.shape[2]
    local_heads = width // HEAD_W
    all_in, all_gate, all_maps, all_out = gather_packed(
        (in_weight, gate_weight, gate_maps, out_weight), "sp", (1, 1, 2, 1)
    )
    for layer in range(LAYERS):
        whole = collect(resid, "tp", 1)
        wide = whole.astype(jnp.float32)
        normed = (
            wide * lax.rsqrt(jnp.mean(wide * wide, axis=1, keepdims=True) + EPS) * norm_gain[layer]
        ).astype(jnp.bfloat16)
        proj_in = jnp.dot(normed, all_in[layer], preferred_element_type=jnp.float32)
        proj_gate = jnp.dot(normed, all_gate[layer], preferred_element_type=jnp.float32)
        xin = proj_in.astype(jnp.bfloat16)
        gin = proj_gate.astype(jnp.bfloat16)
        padded = extended(xin, (("sp", 0),), 2).astype(jnp.float32)
        conv = conv_taps[layer, 0] * padded[0:rows]
        for k in range(1, TAPS):
            conv = conv + conv_taps[layer, k] * padded[k : k + rows]
        conv = conv.astype(jnp.bfloat16)
        stacked = conv.reshape(rows, local_heads, HEAD_W)
        piece = all_maps[layer]
        blocks = piece.reshape(local_heads, HEAD_W, piece.shape[1])
        pre = jnp.einsum("thi,hij->thj", stacked, blocks, preferred_element_type=jnp.float32)
        pre = pre.reshape(rows, local_heads, 4, HEAD_W)
        conv32 = conv.astype(jnp.float32)
        locals_a = []
        locals_h = []
        for direction in range(2):
            rate = jax.nn.sigmoid(pre[:, :, 2 * direction]).reshape(rows, width)
            inp = jax.nn.sigmoid(pre[:, :, 2 * direction + 1]).reshape(rows, width)
            log_a = -8.0 * rate * jax.nn.softplus(-decay_logit[layer, direction])
            decay = jnp.exp(log_a)
            drive = jnp.sqrt(-jnp.expm1(2.0 * log_a)) * inp * conv32
            prod_a, state = lax.associative_scan(
                combine_pair, (decay, drive), reverse=direction == 1, axis=0
            )
            locals_a.append(prod_a)
            locals_h.append(state)
        ones = jnp.ones((width,), jnp.float32)
        zeros = jnp.zeros((width,), jnp.float32)
        _, carry_f = carried_in(
            (locals_a[0][-1], locals_h[0][-1]), "sp", combine_pair, (ones, zeros), False
        )
        _, carry_b = carried_in(
            (locals_a[1][0], locals_h[1][0]), "sp", combine_pair, (ones, zeros), True
        )
        hidden = locals_h[0] + locals_a[0] * carry_f + locals_h[1] + locals_a[1] * carry_b
        mix = (jax.nn.gelu(gin.astype(jnp.float32)) * hidden).astype(jnp.bfloat16)
        full_mix = collect(mix, "tp", 1)
        out = jnp.dot(full_mix, all_out[layer], preferred_element_type=jnp.float32)
        resid = (resid.astype(jnp.float32) + out).astype(jnp.bfloat16)
    wide = resid.astype(jnp.float32)
    total = over_copies(jnp.sum(wide * wide, axis=1), "tp")
    scale = lax.rsqrt(total / D + EPS)
    return (wide * scale[:, None] * final_gain).astype(jnp.bfloat16)


def solution(mesh):
    placed = (
        P(("grp", "sp"), "tp"),
        P(),
        P(None, "sp", "tp"),
        P(None, "sp", "tp"),
        P(None, None, "tp"),
        P(None, None, "tp"),
        P(None, "tp", "sp"),
        P(None, "sp", "tp"),
        P("tp"),
    )
    return jax.shard_map(
        body, mesh=mesh, in_specs=placed, out_specs=P(("grp", "sp"), "tp"), check_vma=False
    )
```

profile of v0, /device:TPU:80, one launch (start us, length us, event | category | flops | bytes accessed | tf_op | source)
XLA Modules:
  0.0 374.0 jit_solution(14561265810740460979)
XLA Ops:
  6.6 0.9 copy.108
  7.5 0.9 copy.109
  8.4 0.9 copy.110
  9.3 0.9 copy.70
  10.3 0.7 pad_maximum_fusion
  11.1 1.0 copy.69
  12.0 0.9 broadcast_in_dim.106
  12.9 7.3 %all-to-all-start = ((bf16[8,128,256]{1,2,0:T(8,128)(2,1)}), bf16[8,128,256]{1,2,0:T(8,128)(2,1)S(1)}, u32[]{:S(2)}, u32[]{:S(2)}) async-start(bf16[8,128,256]{1,2,0:T(8,128)(2,1)} %broadcast_in_dim.106), calls=%async_computation | async-start | bytes 1048576 | tf_op jit(solution)/shard_map/all_to_all | solution.py:33
  23.2 14.6 %all-to-all-done = bf16[8,128,256]{1,2,0:T(8,128)(2,1)S(1)} async-done(((bf16[8,128,256]{1,2,0:T(8,128)(2,1)}), bf16[8,128,256]{1,2,0:T(8,128)(2,1)S(1)}, u32[]{:S(2)}, u32[]{:S(2)}) %all-to-all-start) | async-done | bytes 524320 | tf_op jit(solution)/shard_map/all_to_all | solution.py:33
  38.4 85.1 %all-gather.3.cloned.1.call-done = bf16[3670016]{0:T(1024)(128)(2,1)} async-done(((bf16[114688]{0:T(1024)(128)(2,1)}), bf16[3670016]{0:T(1024)(128)(2,1)}) %all-gather.3.cloned.1.call-update) | async-done | bytes 7340048 | tf_op jit(solution)/shard_map/all_gather | solution.py:23
  123.5 7.9 %reshape.398 = bf16[32,114688]{1,0:T(8,128)(2,1)} reshape(bf16[3670016]{0:T(1024)(128)(2,1)} %all-gather.3.cloned.1.call-done) | data formatting | bytes 14680064 | tf_op jit(solution)/shard_map/all_gather | solution.py:23
  131.4 4.6 %fusion.88 = (bf16[32,32768]{1,0:T(8,128)(2,1)}, bf16[32,32768]{1,0:T(8,128)(2,1)S(1)}, bf16[32,32768]{1,0:T(8,128)(2,1)S(1)}) fusion(bf16[32,114688]{1,0:T(8,128)(2,1)} %reshape.398), kind=kLoop, calls=%fused_computation.336 | loop fusion | bytes 12582912 | tf_op jit(solution)/shard_map/slice | solution.py:25
  136.4 1.1 fusion.91
  138.0 2.2 collective-permute-start
  140.1 1.3 collective-permute-start.1
  141.5 1.8 copy.111
  143.3 4.4 %reshape.381 = bf16[32,2,256,32]{3,2,1,0:T(8,128)(2,1)} reshape(bf16[32,16384]{1,0:T(8,128)(2,1)S(1)} %slice-done) | data formatting | bytes 2097152 | tf_op jit(solution)/shard_map/reshape | solution.py:25
  147.7 4.2 %fusion.89 = (bf16[1,256,32,32]{3,1,0,2:T(8,128)(2,1)S(1)}, bf16[1,256,32,32]{3,1,0,2:T(8,128)(2,1)}) fusion(bf16[2,256,32,32]{3,1,0,2:T(8,128)(2,1)} %bitcast.155), kind=kLoop, calls=%fused_computation.337 | loop fusion | bytes 2097152 | tf_op jit(solution)/shard_map/slice | solution.py:137
  151.8 1.6 fusion.92
  153.4 1.9 copy.71
  155.9 0.8 copy.93
  156.7 0.8 copy.97
  157.4 1.3 convert_multiply_fusion.7
  174.7 0.7 pad.347
  175.4 0.7 pad_maximum_fusion.42
  176.2 0.7 pad_maximum_fusion.34
  176.9 0.7 pad_maximum_fusion.33
  177.6 0.7 fusion.63
  178.3 0.7 pad_maximum_fusion.26
  179.0 0.7 pad_maximum_fusion.25
  179.7 0.7 fusion.59
  183.0 12.4 %all-to-all-start.1 = ((f32[32,2,256]{2,1,0:T(2,128)}), f32[32,2,256]{2,1,0:T(2,128)}, u32[]{:S(2)}, u32[]{:S(2)}) async-start(f32[32,2,256]{2,1,0:T(2,128)} %broadcast_in_dim.108), calls=%async_computation.1 | async-start | bytes 131072 | tf_op jit(solution)/shard_map/all_to_all | solution.py:33
  195.4 0.9 pad_maximum_fusion.4
  196.4 0.9 pad.399
  197.2 0.7 add.843
  197.9 1.5 rev.9
  199.4 0.7 pad_maximum_fusion.46
  200.1 9.0 %all-to-all-done.1 = f32[32,2,256]{2,1,0:T(2,128)} async-done(((f32[32,2,256]{2,1,0:T(2,128)}), f32[32,2,256]{2,1,0:T(2,128)}, u32[]{:S(2)}, u32[]{:S(2)}) %all-to-all-start.1) | async-done | bytes 65568 | tf_op jit(solution)/shard_map/all_to_all | solution.py:33
  209.8 5.0 %all-to-all-start.2 = ((f32[32,2,256]{2,1,0:T(2,128)}), f32[32,2,256]{2,1,0:T(2,128)S(1)}, u32[]{:S(2)}, u32[]{:S(2)}) async-start(f32[32,2,256]{2,1,0:T(2,128)} %broadcast_in_dim.112), calls=%async_computation.2 | async-start | bytes 131072 | tf_op jit(solution)/shard_map/all_to_all | solution.py:33
  214.8 1.0 fusion.98
  216.8 11.4 %all-to-all-done.2 = f32[32,2,256]{2,1,0:T(2,128)S(1)} async-done(((f32[32,2,256]{2,1,0:T(2,128)}), f32[32,2,256]{2,1,0:T(2,128)S(1)}, u32[]{:S(2)}, u32[]{:S(2)}) %all-to-all-start.2) | async-done | bytes 65568 | tf_op jit(solution)/shard_map/all_to_all | solution.py:33
  228.3 0.7 fusion.50
  229.7 1.6 fusion.19
  231.4 0.9 broadcast_in_dim.113
  232.3 6.7 %all-to-all-start.3 = ((bf16[8,128,256]{1,2,0:T(8,128)(2,1)}), bf16[8,128,256]{1,2,0:T(8,128)(2,1)}, u32[]{:S(2)}, u32[]{:S(2)}) async-start(bf16[8,128,256]{1,2,0:T(8,128)(2,1)} %broadcast_in_dim.113), calls=%async_computation.3 | async-start | bytes 1048576 | tf_op jit(solution)/shard_map/all_to_all | solution.py:33
  239.0 2.1 copy.113
  241.1 1.1 fusion.90
  242.2 13.7 %all-to-all-done.3 = bf16[8,128,256]{1,2,0:T(8,128)(2,1)} async-done(((bf16[8,128,256]{1,2,0:T(8,128)(2,1)}), bf16[8,128,256]{1,2,0:T(8,128)(2,1)}, u32[]{:S(2)}, u32[]{:S(2)}) %all-to-all-start.3) | async-done | bytes 524320 | tf_op jit(solution)/shard_map/all_to_all | solution.py:33
  256.0 1.4 fusion
  257.5 0.9 broadcast_in_dim.114
  258.4 3.8 %all-to-all-start.4 = ((bf16[8,128,256]{1,2,0:T(8,128)(2,1)}), bf16[8,128,256]{1,2,0:T(8,128)(2,1)S(1)}, u32[]{:S(2)}, u32[]{:S(2)}) async-start(bf16[8,128,256]{1,2,0:T(8,128)(2,1)} %broadcast_in_dim.114), calls=%async_computation.4 | async-start | bytes 1048576 | tf_op jit(solution)/shard_map/all_to_all | solution.py:33
  262.2 16.1 %all-to-all-done.4 = bf16[8,128,256]{1,2,0:T(8,128)(2,1)S(1)} async-done(((bf16[8,128,256]{1,2,0:T(8,128)(2,1)}), bf16[8,128,256]{1,2,0:T(8,128)(2,1)S(1)}, u32[]{:S(2)}, u32[]{:S(2)}) %all-to-all-start.4) | async-done | bytes 524320 | tf_op jit(solution)/shard_map/all_to_all | solution.py:33
  279.0 1.6 convolution_convert_fusion
  280.6 1.3 collective-permute-start.2
  281.9 1.3 collective-permute-start.3
  283.3 0.8 copy.81
  284.1 1.2 collective-permute-done.3
  291.4 10.6 %all-to-all-start.5 = ((f32[32,2,256]{2,1,0:T(2,128)}), f32[32,2,256]{2,1,0:T(2,128)S(1)}, u32[]{:S(2)}, u32[]{:S(2)}) async-start(f32[32,2,256]{2,1,0:T(2,128)} %broadcast_in_dim.115), calls=%async_computation.5 | async-start | bytes 131072 | tf_op jit(solution)/shard_map/all_to_all | solution.py:33
  302.3 13.4 %all-to-all-done.5 = f32[32,2,256]{2,1,0:T(2,128)S(1)} async-done(((f32[32,2,256]{2,1,0:T(2,128)}), f32[32,2,256]{2,1,0:T(2,128)S(1)}, u32[]{:S(2)}, u32[]{:S(2)}) %all-to-all-start.5) | async-done | bytes 65568 | tf_op jit(solution)/shard_map/all_to_all | solution.py:33
  316.3 4.8 %all-to-all-start.6 = ((f32[32,2,256]{2,1,0:T(2,128)}), f32[32,2,256]{2,1,0:T(2,128)S(1)}, u32[]{:S(2)}, u32[]{:S(2)}) async-start(f32[32,2,256]{2,1,0:T(2,128)} %broadcast_in_dim.116), calls=%async_computation.6 | async-start | bytes 131072 | tf_op jit(solution)/shard_map/all_to_all | solution.py:33
  321.6 13.1 %all-to-all-done.6 = f32[32,2,256]{2,1,0:T(2,128)S(1)} async-done(((f32[32,2,256]{2,1,0:T(2,128)}), f32[32,2,256]{2,1,0:T(2,128)S(1)}, u32[]{:S(2)}, u32[]{:S(2)}) %all-to-all-start.6) | async-done | bytes 65568 | tf_op jit(solution)/shard_map/all_to_all | solution.py:33
  336.2 19.7 %all_to_all.46 = bf16[8,128,256]{1,2,0:T(8,128)(2,1)S(1)} all-to-all(bf16[8,128,256]{1,2,0:T(8,128)(2,1)S(1)} %broadcast_in_dim.117), channel_id=1, replica_groups=mesh['grp'=2,'sp'=32,'tp'=8] {'tp'}, dimensions={0} | all-to-all | bytes 1048576 | tf_op jit(solution)/shard_map/all_to_all | solution.py:33
  356.3 10.1 %all_to_all.47 = f32[8,1,128]{2,1,0:T(1,128)S(1)} all-to-all(f32[8,1,128]{2,1,0:T(1,128)S(1)} %broadcast_in_dim.118), channel_id=1, replica_groups=mesh['grp'=2,'sp'=32,'tp'=8] {'tp'}, dimensions={0} | all-to-all | bytes 8192 | tf_op jit(solution)/shard_map/all_to_all | solution.py:33
  366.4 0.7 multiply_convert_fusion
  (642 shorter events, 34.3 us)
Async XLA Ops:
  6.5 13.7 %copy-start.5 = (f32[2,2048]{1,0:T(2,128)S(1)}, f32[2,2048]{1,0:T(2,128)}, u32[]{:S(2)}) copy-start(f32[2,2048]{1,0:T(2,128)} %param.10) | copy-start | bytes 49156
  6.5 14.8 %copy-start.20 = (f32[2,2,256]{2,1,0:T(2,128)S(1)}, f32[2,2,256]{2,1,0:T(2,128)}, u32[]{:S(2)}) copy-start(f32[2,2,256]{2,1,0:T(2,128)} %param.14) | copy-start | bytes 12292
  6.6 16.0 %copy-start.14 = (f32[2,4,256]{2,1,0:T(4,128)S(1)}, f32[2,4,256]{2,1,0:T(4,128)}, u32[]{:S(2)}) copy-start(f32[2,4,256]{2,1,0:T(4,128)} %param.13) | copy-start | bytes 24580
  6.6 116.9 %all-gather.3.cloned.1.call-start = ((), (), s32[]{:S(2)}) async-start(), calls=%async_computation.9 | async-start | bytes 7569408 | tf_op jit(solution)/shard_map/all_gather | solution.py:23
  12.9 24.9 %all-to-all-start = ((bf16[8,128,256]{1,2,0:T(8,128)(2,1)}), bf16[8,128,256]{1,2,0:T(8,128)(2,1)S(1)}, u32[]{:S(2)}, u32[]{:S(2)}) async-start(bf16[8,128,256]{1,2,0:T(8,128)(2,1)} %broadcast_in_dim.106), calls=%async_computation | async-start | bytes 1048576 | tf_op jit(solution)/shard_map/all_to_all | solution.py:33
  23.1 132.2 %copy-start.10 = (f32[1,1,256]{2,1,0:T(1,128)}, f32[1,1,256]{2,1,0:T(1,128)S(1)}, u32[]{:S(2)}) copy-start(f32[1,1,256]{2,1,0:T(1,128)S(1)} %get-tuple-element.120) | copy-start | bytes 3076
  23.1 132.2 %copy-start.11 = (f32[1,1,256]{2,1,0:T(1,128)}, f32[1,1,256]{2,1,0:T(1,128)S(1)}, u32[]{:S(2)}) copy-start(f32[1,1,256]{2,1,0:T(1,128)S(1)} %get-tuple-element.121) | copy-start | bytes 3076
  23.1 132.2 %copy-start.12 = (f32[1,1,256]{2,1,0:T(1,128)}, f32[1,1,256]{2,1,0:T(1,128)S(1)}, u32[]{:S(2)}) copy-start(f32[1,1,256]{2,1,0:T(1,128)S(1)} %get-tuple-element.122) | copy-start | bytes 3076
  23.1 132.2 %copy-start.13 = (f32[1,1,256]{2,1,0:T(1,128)}, f32[1,1,256]{2,1,0:T(1,128)S(1)}, u32[]{:S(2)}) copy-start(f32[1,1,256]{2,1,0:T(1,128)S(1)} %get-tuple-element.123) | copy-start | bytes 3076
  138.0 17.3 %collective-permute-start = (bf16[2,256]{1,0:T(2,128)(2,1)S(1)}, bf16[2,256]{1,0:T(2,128)(2,1)S(1)}, u32[]{:S(2)}, u32[]{:S(2)}) collective-permute-start(bf16[2,256]{1,0:T(2,128)(2,1)S(1)} %get-tuple-element.64), channel_id=1, source_target_pairs={{0,8},{8,16},{16,24},{24,32},{32,40},{40,48},{48,56},{56,64},{64,7... | collective-permute-start | bytes 3080 | tf_op jit(solution)/shard_map/ppermute | solution.py:49
  140.1 15.1 %collective-permute-start.1 = (bf16[2,256]{1,0:T(2,128)(2,1)S(1)}, bf16[2,256]{1,0:T(2,128)(2,1)S(1)}, u32[]{:S(2)}, u32[]{:S(2)}) collective-permute-start(bf16[2,256]{1,0:T(2,128)(2,1)S(1)} %get-tuple-element.65), channel_id=1, source_target_pairs={{8,0},{16,8},{24,16},{32,24},{40,32},{48,40},{56,48},{64,56},{72,6... | collective-permute-start | bytes 3080 | tf_op jit(solution)/shard_map/ppermute | solution.py:50
  141.5 1.8 slice-start
  147.7 4.2 %copy-start = (bf16[4,8,128,256]{3,2,1,0:T(8,128)(2,1)S(1)}, bf16[4,8,128,256]{3,2,1,0:T(8,128)(2,1)}, u32[]{:S(2)}) copy-start(bf16[4,8,128,256]{3,2,1,0:T(8,128)(2,1)} %copy.111) | copy-start | bytes 6291460
  171.5 3.9 %copy-start.15 = (f32[2,256]{1,0:T(2,128)S(1)}, f32[2,256]{1,0:T(2,128)}, u32[]{:S(2)}) copy-start(f32[2,256]{1,0:T(2,128)} %pad_add_fusion.6) | copy-start | bytes 6148
  172.4 9.5 %copy-start.4 = (f32[31,256]{1,0:T(8,128)S(1)}, f32[31,256]{1,0:T(8,128)}, u32[]{:S(2)}) copy-start(f32[31,256]{1,0:T(8,128)} %slice.1329) | copy-start | bytes 95236
  172.5 9.4 %copy-start.19 = (f32[1,256]{1,0:T(1,128)S(1)}, f32[1,256]{1,0:T(1,128)}, u32[]{:S(2)}) copy-start(f32[1,256]{1,0:T(1,128)} %slice.1754) | copy-start | bytes 3076
  172.6 9.4 %copy-start.18 = (f32[1,256]{1,0:T(1,128)S(1)}, f32[1,256]{1,0:T(1,128)}, u32[]{:S(2)}) copy-start(f32[1,256]{1,0:T(1,128)} %slice.1731) | copy-start | bytes 3076
  174.0 8.1 %copy-start.17 = (f32[1,256]{1,0:T(1,128)S(1)}, f32[1,256]{1,0:T(1,128)}, u32[]{:S(2)}) copy-start(f32[1,256]{1,0:T(1,128)} %slice.1753) | copy-start | bytes 3076
  174.0 8.2 %copy-start.16 = (f32[1,256]{1,0:T(1,128)S(1)}, f32[1,256]{1,0:T(1,128)}, u32[]{:S(2)}) copy-start(f32[1,256]{1,0:T(1,128)} %slice.1730) | copy-start | bytes 3076
  183.0 26.2 %all-to-all-start.1 = ((f32[32,2,256]{2,1,0:T(2,128)}), f32[32,2,256]{2,1,0:T(2,128)}, u32[]{:S(2)}, u32[]{:S(2)}) async-start(f32[32,2,256]{2,1,0:T(2,128)} %broadcast_in_dim.108), calls=%async_computation.1 | async-start | bytes 131072 | tf_op jit(solution)/shard_map/all_to_all | solution.py:33
  209.8 18.4 %all-to-all-start.2 = ((f32[32,2,256]{2,1,0:T(2,128)}), f32[32,2,256]{2,1,0:T(2,128)S(1)}, u32[]{:S(2)}, u32[]{:S(2)}) async-start(f32[32,2,256]{2,1,0:T(2,128)} %broadcast_in_dim.112), calls=%async_computation.2 | async-start | bytes 131072 | tf_op jit(solution)/shard_map/all_to_all | solution.py:33
  232.3 23.6 %all-to-all-start.3 = ((bf16[8,128,256]{1,2,0:T(8,128)(2,1)}), bf16[8,128,256]{1,2,0:T(8,128)(2,1)}, u32[]{:S(2)}, u32[]{:S(2)}) async-start(bf16[8,128,256]{1,2,0:T(8,128)(2,1)} %broadcast_in_dim.113), calls=%async_computation.3 | async-start | bytes 1048576 | tf_op jit(solution)/shard_map/all_to_all | solution.py:33
  241.1 14.9 %copy-start.3 = (bf16[128,256]{1,0:T(8,128)(2,1)S(1)}, bf16[128,256]{1,0:T(8,128)(2,1)}, u32[]{:S(2)}) copy-start(bf16[128,256]{1,0:T(8,128)(2,1)} %param.9) | copy-start | bytes 196612
  258.4 24.9 %copy-start.21 = (f32[1,1,256]{2,1,0:T(1,128)S(1)}, f32[1,1,256]{2,1,0:T(1,128)}, u32[]{:S(2)}) copy-start(f32[1,1,256]{2,1,0:T(1,128)} %get-tuple-element.150) | copy-start | bytes 3076
  258.4 24.9 %copy-start.22 = (f32[1,1,256]{2,1,0:T(1,128)S(1)}, f32[1,1,256]{2,1,0:T(1,128)}, u32[]{:S(2)}) copy-start(f32[1,1,256]{2,1,0:T(1,128)} %get-tuple-element.153) | copy-start | bytes 3076
  258.4 20.0 %all-to-all-start.4 = ((bf16[8,128,256]{1,2,0:T(8,128)(2,1)}), bf16[8,128,256]{1,2,0:T(8,128)(2,1)S(1)}, u32[]{:S(2)}, u32[]{:S(2)}) async-start(bf16[8,128,256]{1,2,0:T(8,128)(2,1)} %broadcast_in_dim.114), calls=%async_computation.4 | async-start | bytes 1048576 | tf_op jit(solution)/shard_map/all_to_all | solution.py:33
  279.0 6.4 %copy-start.6 = (f32[1,1,256]{2,1,0:T(1,128)S(1)}, f32[1,1,256]{2,1,0:T(1,128)}, u32[]{:S(2)}) copy-start(f32[1,1,256]{2,1,0:T(1,128)} %get-tuple-element.118) | copy-start | bytes 3076
  279.0 6.4 %copy-start.7 = (f32[1,1,256]{2,1,0:T(1,128)S(1)}, f32[1,1,256]{2,1,0:T(1,128)}, u32[]{:S(2)}) copy-start(f32[1,1,256]{2,1,0:T(1,128)} %get-tuple-element.119) | copy-start | bytes 3076
  279.0 6.4 %copy-start.8 = (f32[1,1,256]{2,1,0:T(1,128)S(1)}, f32[1,1,256]{2,1,0:T(1,128)}, u32[]{:S(2)}) copy-start(f32[1,1,256]{2,1,0:T(1,128)} %get-tuple-element.124) | copy-start | bytes 3076
  279.0 6.4 %copy-start.9 = (f32[1,1,256]{2,1,0:T(1,128)S(1)}, f32[1,1,256]{2,1,0:T(1,128)}, u32[]{:S(2)}) copy-start(f32[1,1,256]{2,1,0:T(1,128)} %get-tuple-element.125) | copy-start | bytes 3076
  280.6 3.5 collective-permute-start.2
  281.9 3.4 collective-permute-start.3
  290.4 30.8 %copy-start.24 = (pred[32]{0:T(512)(128)(4,1)S(1)}, pred[32]{0:T(512)(128)(4,1)}, u32[]{:S(2)}) copy-start(pred[32]{0:T(512)(128)(4,1)} %iota_compare_fusion.1) | copy-start | bytes 100
  290.5 44.3 %copy-start.23 = (pred[32]{0:T(512)(128)(4,1)S(1)}, pred[32]{0:T(512)(128)(4,1)}, u32[]{:S(2)}) copy-start(pred[32]{0:T(512)(128)(4,1)} %iota_compare_fusion) | copy-start | bytes 100
  290.6 44.9 %copy-start.1 = (bf16[1,32,64,256]{3,2,0,1:T(8,128)(2,1)S(1)}, bf16[1,32,64,256]{3,2,0,1:T(8,128)(2,1)}, u32[]{:S(2)}) copy-start(bf16[1,32,64,256]{3,2,0,1:T(8,128)(2,1)} %get-tuple-element.16) | copy-start | bytes 3145732
  291.4 24.3 %all-to-all-start.5 = ((f32[32,2,256]{2,1,0:T(2,128)}), f32[32,2,256]{2,1,0:T(2,128)S(1)}, u32[]{:S(2)}, u32[]{:S(2)}) async-start(f32[32,2,256]{2,1,0:T(2,128)} %broadcast_in_dim.115), calls=%async_computation.5 | async-start | bytes 131072 | tf_op jit(solution)/shard_map/all_to_all | solution.py:33
  316.3 18.4 %all-to-all-start.6 = ((f32[32,2,256]{2,1,0:T(2,128)}), f32[32,2,256]{2,1,0:T(2,128)S(1)}, u32[]{:S(2)}, u32[]{:S(2)}) async-start(f32[32,2,256]{2,1,0:T(2,128)} %broadcast_in_dim.116), calls=%async_computation.6 | async-start | bytes 131072 | tf_op jit(solution)/shard_map/all_to_all | solution.py:33
  335.5 20.3 %copy-start.2 = (bf16[1,32,64,256]{3,2,0,1:T(8,128)(2,1)S(1)}, bf16[1,32,64,256]{3,2,0,1:T(8,128)(2,1)}, u32[]{:S(2)}) copy-start(bf16[1,32,64,256]{3,2,0,1:T(8,128)(2,1)} %get-tuple-element.12) | copy-start | bytes 3145732
  336.0 30.5 %copy-start.25 = (f32[256]{0:T(256)S(1)}, f32[256]{0:T(256)}, u32[]{:S(2)}) copy-start(f32[256]{0:T(256)} %param.17) | copy-start | bytes 3076
Sparse Core Ops, SparseCore 0:
  11.2 112.2 all-gather.2
where the time goes:
time: 376 us; the launch traced here: 374 us
  waiting for transfers between devices  178 us (47%)
  local copies, waits for them, and re-layouts  65.2 us (17%)
  starting transfers between devices  56.7 us (15%)
  blocking collectives  29.8 us (8%)
  other arithmetic  21.8 us (6%)
  between operations  16.3 us (4%)
  matrix products  6.52 us (2%)
    all_to_all x7, waiting for transfers between devices, from_everyone(): lax.all_to_all(jnp.broadcast_to(value[None], (devices, *value.shape)), ax...  91.4 us
    all_gather x1, waiting for transfers between devices, gather_packed(): lines, at, outs = (lax.all_gather(flat, axis), 0, [])  85.1 us
    all_to_all x7, starting transfers between devices, from_everyone(): lax.all_to_all(jnp.broadcast_to(value[None], (devices, *value.shape)), ax...  50.6 us
    all_to_all x2, blocking collectives, from_everyone(): lax.all_to_all(jnp.broadcast_to(value[None], (devices, *value.shape)), ax...  29.8 us
    slice x188, local copies, waits for them, and re-layouts, body(): lax.associative_scan(combine_pair, (decay, drive), reverse=direction == 1...  13 us
    unnamed x68, local copies, waits for them, and re-layouts  11.1 us
    all_gather x1, local copies, waits for them, and re-layouts, gather_packed(): lines, at, outs = (lax.all_gather(flat, axis), 0, [])  7.88 us
  transfers between devices with their start and end apart: 12, of which 9 were waited for; matrix products, arithmetic and copies ran while one was open for 8% of the time, Pallas kernels for 0%

commit v1 on v0

v1 whole, which is shorter than its diff:
```python
import functools

import jax
import jax.numpy as jnp
from jax import lax
from jax.experimental import pallas as pl
from jax.experimental.pallas import tpu as pltpu
from jax.sharding import PartitionSpec as P

HEAD_W = 256
TAPS = 4
LAYERS = 2
EPS = 1e-06
F32 = jnp.float32
BF16 = jnp.bfloat16


def remote(src, dst, send, recv, where):
    return pltpu.make_async_remote_copy(
        src_ref=src,
        dst_ref=dst,
        send_sem=send,
        recv_sem=recv,
        device_id=where,
        device_id_type=pl.DeviceIdType.MESH,
    )


def bytes_of(ref, sem):
    return pltpu.make_async_copy(ref, ref, sem)


def softplus_small(x):
    y = jnp.exp(-jnp.abs(x))
    series = y * (1 - y * (1 / 2 - y * (1 / 3 - y * (1 / 4 - y * (1 / 5 - y * (1 / 6))))))
    return jnp.maximum(x, 0.0) + jnp.where(y < 0.05, series, jnp.log(1.0 + y))


def neg_expm1(x):
    tail = 1 + x * (1 / 6) * (1 + x * (1 / 7) * (1 + x * (1 / 8)))
    series = x * (1 + x * (1 / 2) * (1 + x * (1 / 3) * (1 + x * (1 / 4) * (1 + x * (1 / 5) * tail))))
    return -jnp.where(x > -0.5, series, jnp.exp(x) - 1.0)


class Ring:
    def __init__(self, held, sems, size, place):
        self.held, self.place, self.size = held, place, size
        self.send, self.recv, self.push_send, self.push_recv = sems
        self.chips = size // 2
        self.half = self.chips // 2
        self.chip, self.core = place // 2, lax.rem(place, 2)
        self.rows = held.shape[1]

    def slot(self, chip):
        return lax.rem(chip + 2 * self.chips, self.chips) * 2 + self.core

    def view(self, slot, flow, step):
        if step < self.half:
            return self.held.at[slot]
        rows = self.rows // 2
        return self.held.at[slot, pl.ds(flow * rows, rows)]

    def hop(self, flow, step):
        way = 1 - 2 * flow
        view = self.view(self.slot(self.chip - way * (step - 1)), flow, step)
        return remote(
            view, view, self.send, self.recv.at[flow, step - 1], {"sp": self.slot(self.chip + way)}
        )

    def landed(self, flow, step):
        way = 1 - 2 * flow
        view = self.view(self.slot(self.chip - way * step), flow, step)
        return remote(
            view, view, self.send, self.recv.at[flow, step - 1], {"sp": self.slot(self.chip + way)}
        )

    def push(self, slot):
        view = self.held.at[slot]
        other = self.chip * 2 + 1 - self.core
        remote(view, view, self.push_send, self.push_recv, {"sp": other}).start()

    def begin(self):
        for flow in range(2):
            self.hop(flow, 1).start()
        self.push(self.place)

    def step(self, step):
        for flow in range(2):
            self.landed(flow, step).wait_recv()
            if step < self.half:
                self.hop(flow, step + 1).start()
                way = 1 - 2 * flow
                self.push(self.slot(self.chip - way * step))
        if step == self.half:
            self.push(self.slot(self.chip + self.half))

    def joined(self):
        bytes_of(self.held.at[pl.ds(0, self.chips)], self.push_recv).wait()

    def drain(self):
        bytes_of(self.held.at[pl.ds(0, self.chips - 1)], self.send).wait()
        bytes_of(self.held.at[pl.ds(0, self.chips)], self.push_send).wait()


class Spread:
    def __init__(self, held, send, recv, size, place):
        self.held, self.send, self.recv = held, send, recv
        self.size, self.place = size, place
        self.order = sorted(range(1, size), key=lambda d: -min(d, size - d))

    def begin(self, block):
        for d in self.order:
            peer = lax.rem(self.place + d, self.size)
            remote(
                block, self.held.at[self.place], self.send, self.recv.at[d - 1], {"tp": peer}
            ).start()

    def wait(self):
        for d in self.order:
            slot = self.held.at[lax.rem(self.place + self.size - d, self.size)]
            remote(slot, slot, self.send, self.recv.at[d - 1], {"tp": self.place}).wait_recv()

    def drain(self):
        bytes_of(self.held.at[pl.ds(0, self.size - 1)], self.send).wait()


def kernel(
    S,
    T,
    tokens,
    norm_gain,
    in_weight,
    gate_weight,
    conv_taps,
    decay_logit,
    gate_maps,
    out_weight,
    final_gain,
    out,
    held_a,
    held_b,
    held_c,
    acts,
    edges,
    edge_in,
    padded,
    coef,
    local,
    hidden,
    gated,
    msg,
    carries,
    block,
    squares,
    ring_recv,
    ring_send,
    x_recv,
    x_send,
    edge_sems,
    carry_sems,
    square_sems,
):
    p = lax.axis_index("sp")
    t = lax.axis_index("tp")
    rows, width = tokens.shape
    depth = in_weight.shape[1]
    cols = gate_maps.shape[2]
    seg = rows // 8
    share = width // depth
    quarter = S // 4

    barrier = pltpu.get_barrier_semaphore()
    for d in range(1, T):
        pl.semaphore_signal(
            barrier, inc=1, device_id={"tp": lax.rem(t + d, T)}, device_id_type=pl.DeviceIdType.MESH
        )
    for d in range(1, S):
        pl.semaphore_signal(
            barrier, inc=1, device_id={"sp": lax.rem(p + d, S)}, device_id_type=pl.DeviceIdType.MESH
        )

    eye = (
        lax.broadcasted_iota(jnp.int32, (cols, cols), 0)
        == lax.broadcasted_iota(jnp.int32, (cols, cols), 1)
    ).astype(BF16)

    def turned(layer):
        return lax.dot_general(
            eye, gate_maps[layer], (((1,), (1,)), ((), ())), preferred_element_type=F32
        ).astype(BF16)

    held_a[p, 0:depth] = in_weight[0]
    held_a[p, depth : depth + cols] = turned(0)
    held_b[p, 0:depth] = gate_weight[0]
    held_b[p, depth : 2 * depth] = out_weight[0]
    held_c[p, 0:depth] = in_weight[1]
    held_c[p, depth : depth + cols] = turned(1)
    held_c[p, depth + cols : 2 * depth + cols] = gate_weight[1]
    held_c[p, 2 * depth + cols : 3 * depth + cols] = out_weight[1]
    acts[0, t] = tokens[...]

    pl.semaphore_wait(barrier, T + S - 2)

    def ring(held, k):
        return Ring(
            held,
            (ring_send.at[k, 0], ring_recv.at[k], ring_send.at[k, 1], ring_send.at[k, 2]),
            S,
            p,
        )

    ring_a, ring_b, ring_c = ring(held_a, 0), ring(held_b, 1), ring(held_c, 2)
    spread = [Spread(acts.at[k], x_send.at[k], x_recv.at[k], T, t) for k in range(4)]

    ring_a.begin()
    spread[0].begin(tokens)
    ring_b.begin()
    for step in range(1, S // 4 + 1):
        ring_a.step(step)
        ring_b.step(step)
    ring_c.begin()
    spread[0].wait()
    ring_a.joined()

    later = iter(range(1, S // 4 + 1))

    def forward_some():
        step = next(later, None)
        if step is not None:
            ring_c.step(step)

    for layer in range(LAYERS):
        if layer == 0:
            in_at, map_at, gate_at, out_at = (held_a, 0), (held_a, depth), (held_b, 0), (held_b, depth)
        else:
            for _ in range(S // 4):
                forward_some()
            ring_c.joined()
            in_at, map_at = (held_c, 0), (held_c, depth)
            gate_at, out_at = (held_c, depth + cols), (held_c, 2 * depth + cols)

        def weight(at, k):
            held, row = at
            return held[k * share : (k + 1) * share, row : row + depth].reshape(width, width)

        full = acts.at[2 * layer]
        total = jnp.zeros((rows, 1), F32)
        for k in range(T):
            wide = full[k].astype(F32)
            total = total + jnp.sum(wide * wide, axis=1, keepdims=True)
        scale = lax.rsqrt(total / (T * width) + EPS)
        proj = jnp.zeros((rows, width), F32)
        for k in range(T):
            wide = full[k].astype(F32)
            normed = (
                wide * scale * norm_gain[layer : layer + 1, k * width : (k + 1) * width]
            ).astype(BF16)
            full[k] = normed
            proj = proj + jnp.dot(normed, weight(in_at, k), preferred_element_type=F32)
        xin = proj.astype(BF16)
        edges[layer, 0] = xin[rows - 16 : rows]
        edges[layer, 1] = xin[0:16]
        up = remote(
            edges.at[layer, 0], edge_in.at[layer, 0], edge_sems.at[layer, 0], edge_sems.at[layer, 1],
            {"sp": lax.rem(p + 1, S)},
        )
        down = remote(
            edges.at[layer, 1], edge_in.at[layer, 1], edge_sems.at[layer, 2], edge_sems.at[layer, 3],
            {"sp": lax.rem(p + S - 1, S)},
        )
        up.start()
        down.start()
        padded[8 : 8 + rows] = xin.astype(F32)
        if layer == 0:
            ring_b.joined()
        forward_some()
        proj = jnp.zeros((rows, width), F32)
        for k in range(T):
            proj = proj + jnp.dot(full[k], weight(gate_at, k), preferred_element_type=F32)
        gated[...] = jax.nn.gelu(proj.astype(BF16).astype(F32))
        up.wait()
        down.wait()
        forward_some()
        before = edge_in[layer, 0].astype(F32)[8:16]
        after = edge_in[layer, 1].astype(F32)[0:8]
        padded[0:8] = jnp.where(p == 0, 0.0, before)
        padded[8 + rows : 16 + rows] = jnp.where(p == S - 1, 0.0, after)
        conv = conv_taps[layer, 0:1] * padded[6 : 6 + rows]
        for k in range(1, TAPS):
            conv = conv + conv_taps[layer, k : k + 1] * padded[6 + k : 6 + k + rows]
        conv = conv.astype(BF16)
        conv32 = conv.astype(F32)

        def gate(g):
            held, row = map_at
            maps = held[g * quarter : (g + 1) * quarter, row : row + cols].reshape(width, width)
            pre = lax.dot_general(
                conv, maps, (((1,), (1,)), ((), ())), preferred_element_type=F32
            )
            return jax.nn.sigmoid(pre)

        first = []
        for way in range(2):
            log_a = (
                -8.0 * gate(2 * way) * softplus_small(-decay_logit[layer, way : way + 1])
            )
            decay = jnp.exp(log_a)
            drive = jnp.sqrt(neg_expm1(2.0 * log_a)) * gate(2 * way + 1) * conv32
            for lane in range(width // 128):
                coef[0, lane] = decay[:, lane * 128 : (lane + 1) * 128]
                coef[1, lane] = drive[:, lane * 128 : (lane + 1) * 128]
            prod = jnp.ones((8, width), F32)
            state = jnp.zeros((8, width), F32)
            for r in range(seg) if way == 0 else reversed(range(seg)):
                a, b = (
                    jnp.concatenate(
                        [coef[k, lane, pl.ds(r, 8, stride=seg), :] for lane in range(width // 128)],
                        axis=1,
                    )
                    for k in range(2)
                )
                state = a * state + b
                prod = a * prod
                local[way, 0, r] = prod
                local[way, 1, r] = state
            run_a = jnp.ones((1, width), F32)
            run_h = jnp.zeros((1, width), F32)
            heads = [None] * 8
            for s in range(8) if way == 0 else reversed(range(8)):
                heads[s] = (run_a, run_h)
                run_h = prod[s : s + 1] * run_h + state[s : s + 1]
                run_a = prod[s : s + 1] * run_a
            msg[layer, way, 0:1] = run_a
            msg[layer, way, 1:2] = run_h
            first.append(
                (
                    jnp.concatenate([h[0] for h in heads], axis=0),
                    jnp.concatenate([h[1] for h in heads], axis=0),
                )
            )

        def tell(d, _):
            remote(
                msg.at[layer, (p + d) // S],
                carries.at[layer, p],
                carry_sems.at[layer, 0],
                carry_sems.at[layer, 1],
                {"sp": lax.rem(p + d, S)},
            ).start()
            return 0

        lax.fori_loop(1, S, tell, 0)
        carries[layer, p] = msg[layer, 0]
        forward_some()
        bytes_of(carries.at[layer, pl.ds(0, S - 1)], carry_sems.at[layer, 1]).wait()

        def fold(j, held):
            ahead, behind = held
            one = carries[layer, j]
            ahead = jnp.where(j < p, one[0:1] * ahead + one[1:2], ahead)
            k = S - 1 - j
            one = carries[layer, k]
            behind = jnp.where(k > p, one[0:1] * behind + one[1:2], behind)
            return ahead, behind

        zero = jnp.zeros((1, width), F32)
        enter = lax.fori_loop(0, S, fold, (zero, zero), unroll=True)
        heads = [a * e + h for (a, h), e in zip(first, enter)]
        for r in range(seg):
            both = (
                local[0, 1, r]
                + local[0, 0, r] * heads[0]
                + local[1, 1, r]
                + local[1, 0, r] * heads[1]
            )
            for lane in range(width // 128):
                hidden[lane, pl.ds(r, 8, stride=seg), :] = both[:, lane * 128 : (lane + 1) * 128]
        states = jnp.concatenate([hidden[lane] for lane in range(width // 128)], axis=1)
        mix = (gated[...] * states).astype(BF16)
        block[layer] = mix
        across = spread[2 * layer + 1]
        acts[2 * layer + 1, t] = mix
        across.begin(block.at[layer])
        forward_some()
        across.wait()
        full = acts.at[2 * layer + 1]
        moved = jnp.zeros((rows, width), F32)
        for k in range(T):
            moved = moved + jnp.dot(full[k], weight(out_at, k), preferred_element_type=F32)
        before = tokens[...] if layer == 0 else block[2]
        resid = (before.astype(F32) + moved).astype(BF16)
        if layer < LAYERS - 1:
            block[2] = resid
            acts[2, t] = resid
            spread[2].begin(block.at[2])
            forward_some()
            spread[2].wait()

    wide = resid.astype(F32)
    own = jnp.sum(wide * wide, axis=1, keepdims=True)
    line = jnp.broadcast_to(own, (rows, rows)).T[0:1]
    squares[t] = line
    for d in range(1, T):
        copy = remote(
            squares.at[t], squares.at[t], square_sems.at[0], square_sems.at[1],
            {"tp": lax.rem(t + d, T)},
        )
        copy.start()
    bytes_of(squares.at[pl.ds(0, T - 1)], square_sems.at[1]).wait()
    total = squares[0]
    for k in range(1, T):
        total = total + squares[k]
    scale = lax.rsqrt(total / (T * width) + EPS)
    scale = jnp.broadcast_to(scale, (rows, rows)).T[:, 0:1]
    out[...] = (wide * scale * final_gain[...]).astype(BF16)

    for each in (ring_a, ring_b, ring_c, *spread):
        each.drain()
    for layer in range(LAYERS):
        bytes_of(carries.at[layer, pl.ds(0, S - 1)], carry_sems.at[layer, 0]).wait()
    bytes_of(squares.at[pl.ds(0, T - 1)], square_sems.at[0]).wait()


def body(S, T, *args):
    tokens, gate_maps, in_weight = args[0], args[6], args[2]
    args = (*args[:-1], args[-1][None])
    rows, width = tokens.shape
    depth = in_weight.shape[1]
    cols = gate_maps.shape[2]
    seg = rows // 8
    vmem = pl.BlockSpec(memory_space=pltpu.VMEM)
    dma = pltpu.SemaphoreType.DMA
    return pl.pallas_call(
        functools.partial(kernel, S, T),
        out_shape=jax.ShapeDtypeStruct((rows, width), BF16),
        in_specs=[vmem] * len(args),
        out_specs=vmem,
        scratch_shapes=[
            pltpu.VMEM((S, depth + cols, width), BF16),
            pltpu.VMEM((S, 2 * depth, width), BF16),
            pltpu.VMEM((S, 3 * depth + cols, width), BF16),
            pltpu.VMEM((4, T, rows, width), BF16),
            pltpu.VMEM((LAYERS, 2, 16, width), BF16),
            pltpu.VMEM((LAYERS, 2, 16, width), BF16),
            pltpu.VMEM((rows + 16, width), F32),
            pltpu.VMEM((2, width // 128, rows, 128), F32),
            pltpu.VMEM((2, 2, seg, 8, width), F32),
            pltpu.VMEM((width // 128, rows, 128), F32),
            pltpu.VMEM((rows, width), F32),
            pltpu.VMEM((LAYERS, 2, 2, width), F32),
            pltpu.VMEM((LAYERS, S, 2, width), F32),
            pltpu.VMEM((3, rows, width), BF16),
            pltpu.VMEM((T, 1, rows), F32),
            dma((3, 2, S // 4)),
            dma((3, 3)),
            dma((4, T - 1)),
            dma((4,)),
            dma((LAYERS, 4)),
            dma((LAYERS, 2)),
            dma((2,)),
        ],
        compiler_params=pltpu.CompilerParams(
            collective_id=0, has_side_effects=True, vmem_limit_bytes=40 * 2**20
        ),
        name="recurrent_layers",
    )(*args)


def solution(mesh):
    placed = (
        P(("grp", "sp"), "tp"),
        P(),
        P(None, "sp", "tp"),
        P(None, "sp", "tp"),
        P(None, None, "tp"),
        P(None, None, "tp"),
        P(None, "tp", "sp"),
        P(None, "sp", "tp"),
        P("tp"),
    )
    return jax.shard_map(
        functools.partial(body, mesh.shape["sp"], mesh.shape["tp"]),
        mesh=mesh,
        in_specs=placed,
        out_specs=P(("grp", "sp"), "tp"),
        check_vma=False,
    )
```

time: 376 us -> 173 us (0.46)
  waiting for transfers between devices: 178 us -> 0 us
  Pallas kernels: 0 us -> 169 us
  local copies, waits for them, and re-layouts: 65.2 us -> 3.29 us
  starting transfers between devices: 56.7 us -> 0 us
  blocking collectives: 29.8 us -> 0 us
  other arithmetic: 21.8 us -> 0 us
  between operations: 16.3 us -> 0.1 us
  matrix products: 6.52 us -> 0 us
    pallas_call x0 -> x1, Pallas kernels: none -> 169 us  [body(): pl.pallas_call(functools.partial(kernel, S, T), out_shape=jax.ShapeDtypeS...]
    all_to_all x7 -> x0, waiting for transfers between devices: 91.4 us -> none  [from_everyone(): lax.all_to_all(jnp.broadcast_to(value[None], (devices, *value.shape)), ax...]
    all_gather x1 -> x0, waiting for transfers between devices: 85.1 us -> none  [gather_packed(): lines, at, outs = (lax.all_gather(flat, axis), 0, [])]
    all_to_all x7 -> x0, starting transfers between devices: 50.6 us -> none  [from_everyone(): lax.all_to_all(jnp.broadcast_to(value[None], (devices, *value.shape)), ax...]
    slice x279 -> x0, local copies, waits for them, and re-layouts: 31.7 us -> none  [the longest x188 13 us: body(): lax.associative_scan(combine_pair, (decay, drive), reverse=direction == 1...]
    all_to_all x2 -> x0, blocking collectives: 29.8 us -> none  [from_everyone(): lax.all_to_all(jnp.broadcast_to(value[None], (devices, *value.shape)), ax...]
    all_gather x1 -> x0, local copies, waits for them, and re-layouts: 7.88 us -> none  [gather_packed(): lines, at, outs = (lax.all_gather(flat, axis), 0, [])]
    unnamed x68 -> x18, local copies, waits for them, and re-layouts: 11.1 us -> 3.29 us
  transfers between devices with their start and end apart: 12 -> 0, of which waited for: 9 -> 0; matrix products, arithmetic and copies ran while one was open for 8% -> 0% of each run, Pallas kernels for 0% -> 0%
where the time goes in v1:
time: 173 us
  Pallas kernels  169 us (98%)
  local copies, waits for them, and re-layouts  3.29 us (2%)
    pallas_call x1, Pallas kernels, body(): pl.pallas_call(functools.partial(kernel, S, T), out_shape=jax.ShapeDtypeS...  169 us

profile of v1, /device:TPU:80, one launch (start us, length us, event | category | flops | bytes accessed | tf_op | source)
XLA Modules:
  0.0 172.6 jit_solution(11165754438270818706)
XLA Ops:
  0.0 0.0 copy-start
  0.0 0.0 copy-start.1
  0.0 0.0 copy-start.4
  0.0 0.0 copy-start.5
  0.0 0.0 copy-start.6
  0.0 0.0 copy-start.7
  0.0 1.0 copy.10.gate_maps
  1.0 0.0 copy-done
  1.0 0.0 copy-done.1
  1.0 0.0 copy-done.4
  1.0 0.0 copy-done.5
  1.0 0.0 copy-done.6
  1.1 0.0 copy-done.7
  1.1 0.0 copy-start.2
  1.1 0.8 copy-done.2
  1.9 0.0 copy-start.3
  1.9 0.8 copy-done.3
  2.8 169.2 %recurrent_layers.1 = bf16[128,256]{1,0:T(8,128)(2,1)S(1)} custom-call(bf16[128,256]{1,0:T(8,128)(2,1)S(1)} %copy-done, f32[2,2048]{1,0:T(2,128)S(1)} %copy-done.4, bf16[2,64,256]{2,1,0:T(8,128)(2,1)S(1)} %copy-done.1, bf16[2,64,256]{2,1,0:T(8,128)(2,1)S(1)} %copy-done.2, f32[2,4,256]{2,1,0:T(4,128)S(1)} %copy-done.5, f32[2,2,256]{2,1,0:T(2,128)S(1)} %copy-done.6, ...), custom_call_target="tpu_custom_call" | custom-call | tf_op jit(solution)/shard_map/recurrent_layers/pallas_call | solution.py:433
  171.9 0.6 copy.12
Async XLA Ops:
  0.0 1.0 copy-start
  0.0 1.0 copy-start.1
  0.0 1.0 copy-start.4
  0.0 1.0 copy-start.5
  0.0 1.0 copy-start.6
  0.0 1.0 copy-start.7
  1.1 0.8 copy-start.2
  1.9 0.8 copy-start.3

commit v2 on v1

v2 whole, which is shorter than its diff:
```python
import functools

import jax
import jax.numpy as jnp
from jax import lax
from jax.experimental import pallas as pl
from jax.experimental.pallas import tpu as pltpu
from jax.sharding import PartitionSpec as P

HEAD_W = 256
TAPS = 4
LAYERS = 2
EPS = 1e-06
F32 = jnp.float32
BF16 = jnp.bfloat16


def remote(src, dst, send, recv, where):
    return pltpu.make_async_remote_copy(
        src_ref=src,
        dst_ref=dst,
        send_sem=send,
        recv_sem=recv,
        device_id=where,
        device_id_type=pl.DeviceIdType.MESH,
    )


def bytes_of(ref, sem):
    return pltpu.make_async_copy(ref, ref, sem)


def softplus_small(x):
    y = jnp.exp(-jnp.abs(x))
    series = y * (1 - y * (1 / 2 - y * (1 / 3 - y * (1 / 4 - y * (1 / 5 - y * (1 / 6))))))
    return jnp.maximum(x, 0.0) + jnp.where(y < 0.05, series, jnp.log(1.0 + y))


def neg_expm1(x):
    tail = 1 + x * (1 / 6) * (1 + x * (1 / 7) * (1 + x * (1 / 8)))
    series = x * (1 + x * (1 / 2) * (1 + x * (1 / 3) * (1 + x * (1 / 4) * (1 + x * (1 / 5) * tail))))
    return -jnp.where(x > -0.5, series, jnp.exp(x) - 1.0)


class Gather:
    def __init__(self, held, sems, axis, size, place, reach, twins):
        self.held, self.axis, self.reach, self.twins = held, axis, reach, twins
        self.send, self.recv = sems[:2]
        self.size = size // 2 if twins else size
        self.half = self.size // 2
        self.own = place
        self.place = place // 2 if twins else place
        self.core = lax.rem(place, 2) if twins else None
        if twins:
            self.push_send, self.push_recv = sems[2:]
        self.rows = held.shape[1]
        self.stages = -(-self.half // reach)
        self.last = self.stages

    def slot(self, place):
        place = lax.rem(place + 2 * self.size, self.size)
        return place * 2 + self.core if self.twins else place

    def view(self, slot, flow, d):
        if d < self.half:
            return self.held.at[slot]
        rows = self.rows // 2
        return self.held.at[slot, pl.ds(flow * rows, rows)]

    def hop(self, flow, d, j):
        way = 1 - 2 * flow
        view = self.view(self.slot(self.place - way * (d - j)), flow, d)
        to = {self.axis: self.slot(self.place + way * j)}
        return remote(view, view, self.send, self.recv.at[flow, d - 1], to)

    def landed(self, flow, d):
        way = 1 - 2 * flow
        view = self.view(self.slot(self.place - way * d), flow, d)
        to = {self.axis: self.slot(self.place + way)}
        remote(view, view, self.send, self.recv.at[flow, d - 1], to).wait_recv()
        if self.twins and d < self.half:
            self.push(self.slot(self.place - way * d))

    def push(self, slot):
        view = self.held.at[slot]
        other = self.place * 2 + 1 - self.core
        remote(view, view, self.push_send, self.push_recv, {self.axis: other}).start()

    def emit(self, stage, flow):
        for j in range(self.reach, 0, -1):
            if self.reach * stage + j <= self.half:
                self.hop(flow, self.reach * stage + j, j).start()

    def begin(self):
        for flow in range(2):
            self.emit(0, flow)
        if self.twins:
            self.push(self.own)

    def step(self, stage):
        ahead = self.reach * stage
        if stage < self.stages:
            for flow in range(2):
                self.landed(flow, ahead)
                self.emit(stage, flow)
        for d in range(ahead - self.reach + 1, min(ahead, self.half) + 1):
            if stage < self.stages and d == ahead:
                continue
            for flow in range(2):
                self.landed(flow, d)
            if self.twins and d == self.half:
                self.push(self.slot(self.place + self.half))

    def wait(self, first=1):
        for stage in range(first, self.stages + 1):
            self.step(stage)

    def joined(self):
        bytes_of(self.held.at[pl.ds(0, self.size)], self.push_recv).wait()

    def drain(self):
        bytes_of(self.held.at[pl.ds(0, self.size - 1)], self.send).wait()
        if self.twins:
            bytes_of(self.held.at[pl.ds(0, self.size)], self.push_send).wait()


REACH_IN = 1
REACH_LATER = 1
REACH_X = 2


def kernel(
    S,
    T,
    tokens_hbm,
    norm_gain_hbm,
    in_weight,
    gate_weight,
    conv_taps_hbm,
    decay_logit_hbm,
    gate_maps,
    out_weight,
    final_gain_hbm,
    out,
    tokens,
    norm_gain,
    conv_taps,
    decay_logit,
    final_gain,
    held_in,
    held_map,
    held_gate,
    held_out,
    held_c,
    held_d,
    acts,
    normed,
    edges,
    edge_in,
    padded,
    coef,
    local,
    hidden,
    gated,
    msg,
    carries,
    block,
    squares,
    load_sems,
    ring_recv,
    ring_send,
    x_recv,
    x_send,
    edge_sems,
    carry_sems,
    square_sems,
):
    p = lax.axis_index("sp")
    t = lax.axis_index("tp")
    rows, width = tokens.shape
    depth = in_weight.shape[1]
    cols = gate_maps.shape[1]
    seg = rows // 8
    share = width // depth
    quarter = S // 4

    held = (held_in, held_map, held_gate, held_out, held_c, held_d)
    rings = [
        Gather(
            g,
            (ring_send.at[k, 0], ring_recv.at[k], ring_send.at[k, 1], ring_send.at[k, 2]),
            "sp",
            S,
            p,
            REACH_IN if k < 2 else REACH_LATER,
            True,
        )
        for k, g in enumerate(held)
    ]
    ring_in, ring_map, ring_gate, ring_out, ring_c, ring_d = rings
    spread = [
        Gather(acts.at[k], (x_send.at[k], x_recv.at[k]), "tp", T, t, REACH_X, False)
        for k in range(4)
    ]

    barrier = pltpu.get_barrier_semaphore()
    friends = [
        {"sp": ring_in.slot(ring_in.place + way * j)}
        for way in (1, -1)
        for j in range(1, REACH_IN + 1)
    ]
    friends.append({"sp": ring_in.place * 2 + 1 - ring_in.core})
    friends.extend({"tp": lax.rem(t + d, T)} for d in range(1, T))
    for friend in friends:
        pl.semaphore_signal(
            barrier, inc=1, device_id=friend, device_id_type=pl.DeviceIdType.MESH
        )

    loads = [
        (in_weight.at[0], held_in.at[p]),
        (gate_maps.at[0], held_map.at[p]),
        (tokens_hbm, tokens),
        (gate_weight.at[0], held_gate.at[p]),
        (out_weight.at[0], held_out.at[p]),
        (in_weight.at[1], held_c.at[p, pl.ds(0, depth)]),
        (gate_maps.at[1], held_c.at[p, pl.ds(depth, cols)]),
        (gate_weight.at[1], held_d.at[p, pl.ds(0, depth)]),
        (out_weight.at[1], held_d.at[p, pl.ds(depth, depth)]),
        (norm_gain_hbm, norm_gain),
        (conv_taps_hbm, conv_taps),
        (decay_logit_hbm, decay_logit),
        (final_gain_hbm, final_gain),
    ]
    loads = [
        pltpu.make_async_copy(src, dst, load_sems.at[k]) for k, (src, dst) in enumerate(loads)
    ]
    for load in loads:
        load.start()
    for load in loads:
        load.wait()
    acts[0, t] = tokens[...]
    with jax.named_scope("w_barrier"):
        pl.semaphore_wait(barrier, len(friends))

    ring_in.begin()
    ring_map.begin()
    spread[0].begin()

    def normalize(layer):
        full = acts.at[2 * layer]
        total = jnp.zeros((rows, 1), F32)
        for k in range(T):
            wide = full[k].astype(F32)
            total = total + jnp.sum(wide * wide, axis=1, keepdims=True)
        scale = lax.rsqrt(total / (T * width) + EPS)
        for k in range(T):
            wide = full[k].astype(F32)
            normed[k] = (
                wide * scale * norm_gain[layer : layer + 1, k * width : (k + 1) * width]
            ).astype(BF16)

    lagged = [ring_gate, ring_out]
    for step in range(1, ring_in.last + 1):
        with jax.named_scope("w_in%d" % step):
            ring_in.step(step)
            ring_map.step(step)
        with jax.named_scope("w_go%d" % step):
            for each in lagged:
                if step == 1:
                    each.begin()
                elif step <= each.last:
                    each.step(step - 1)
        if step == 1:
            with jax.named_scope("w_tok1"):
                spread[0].step(1)
        if step == max(1, ring_in.last - 1):
            with jax.named_scope("w_tokens"):
                spread[0].wait(2)
            normalize(0)
    with jax.named_scope("w_join"):
        ring_in.joined()

    def later(*steps):
        for step in steps:
            with jax.named_scope("w_c%d" % step):
                for each in (ring_c, ring_d):
                    if step == 0:
                        each.begin()
                    elif step <= each.last:
                        each.step(step)

    for layer in range(LAYERS):
        if layer == 0:
            in_at, map_at, gate_at, out_at = (held_in, 0), (held_map, 0), (held_gate, 0), (held_out, 0)
        else:
            in_at, map_at, gate_at, out_at = (held_c, 0), (held_c, depth), (held_d, 0), (held_d, depth)

        def weight(at, k):
            ref, row = at
            return ref[k * share : (k + 1) * share, row : row + depth].reshape(width, width)

        proj = jnp.zeros((rows, width), F32)
        for k in range(T):
            proj = proj + jnp.dot(normed[k], weight(in_at, k), preferred_element_type=F32)
        xin = proj.astype(BF16)
        edges[layer, 0] = xin[rows - 16 : rows]
        edges[layer, 1] = xin[0:16]
        up = remote(
            edges.at[layer, 0], edge_in.at[layer, 0], edge_sems.at[layer, 0], edge_sems.at[layer, 1],
            {"sp": lax.rem(p + 1, S)},
        )
        down = remote(
            edges.at[layer, 1], edge_in.at[layer, 1], edge_sems.at[layer, 2], edge_sems.at[layer, 3],
            {"sp": lax.rem(p + S - 1, S)},
        )
        up.start()
        down.start()
        padded[8 : 8 + rows] = xin.astype(F32)
        if layer == 0:
            with jax.named_scope("w_golast"):
                ring_map.joined()
                for each in lagged:
                    for step in range(min(ring_in.last, each.last), each.last + 1):
                        each.step(step)
            later(0)
        with jax.named_scope("w_halo"):
            up.wait()
            down.wait()
        before = edge_in[layer, 0].astype(F32)[8:16]
        after = edge_in[layer, 1].astype(F32)[0:8]
        padded[0:8] = jnp.where(p == 0, 0.0, before)
        padded[8 + rows : 16 + rows] = jnp.where(p == S - 1, 0.0, after)
        conv = conv_taps[layer, 0:1] * padded[6 : 6 + rows]
        for k in range(1, TAPS):
            conv = conv + conv_taps[layer, k : k + 1] * padded[6 + k : 6 + k + rows]
        conv = conv.astype(BF16)
        conv32 = conv.astype(F32)

        def gate(g):
            ref, row = map_at
            maps = ref[g * quarter : (g + 1) * quarter, row : row + cols].reshape(width, width)
            pre = lax.dot_general(
                conv, maps, (((1,), (1,)), ((), ())), preferred_element_type=F32
            )
            return jax.nn.sigmoid(pre)

        first = []
        for way in range(2):
            log_a = (
                -8.0 * gate(2 * way) * softplus_small(-decay_logit[layer, way : way + 1])
            )
            decay = jnp.exp(log_a)
            drive = jnp.sqrt(neg_expm1(2.0 * log_a)) * gate(2 * way + 1) * conv32
            for lane in range(width // 128):
                coef[0, lane] = decay[:, lane * 128 : (lane + 1) * 128]
                coef[1, lane] = drive[:, lane * 128 : (lane + 1) * 128]
            prod = jnp.ones((8, width), F32)
            state = jnp.zeros((8, width), F32)
            for r in range(seg) if way == 0 else reversed(range(seg)):
                a, b = (
                    jnp.concatenate(
                        [coef[k, lane, pl.ds(r, 8, stride=seg), :] for lane in range(width // 128)],
                        axis=1,
                    )
                    for k in range(2)
                )
                state = a * state + b
                prod = a * prod
                local[way, 0, r] = prod
                local[way, 1, r] = state
            run_a = jnp.ones((1, width), F32)
            run_h = jnp.zeros((1, width), F32)
            heads = [None] * 8
            for s in range(8) if way == 0 else reversed(range(8)):
                heads[s] = (run_a, run_h)
                run_h = prod[s : s + 1] * run_h + state[s : s + 1]
                run_a = prod[s : s + 1] * run_a
            msg[layer, way, 0:1] = run_a
            msg[layer, way, 1:2] = run_h
            first.append(
                (
                    jnp.concatenate([h[0] for h in heads], axis=0),
                    jnp.concatenate([h[1] for h in heads], axis=0),
                )
            )

        def tell(d, _):
            remote(
                msg.at[layer, (p + d) // S],
                carries.at[layer, p],
                carry_sems.at[layer, 0],
                carry_sems.at[layer, 1],
                {"sp": lax.rem(p + d, S)},
            ).start()
            return 0

        lax.fori_loop(1, S, tell, 0)
        carries[layer, p] = msg[layer, 0]
        if layer == 0:
            later(1)
            with jax.named_scope("w_joingate"):
                ring_gate.joined()
        else:
            with jax.named_scope("w_joind"):
                ring_d.joined()
        proj = jnp.zeros((rows, width), F32)
        for k in range(T):
            proj = proj + jnp.dot(normed[k], weight(gate_at, k), preferred_element_type=F32)
        gated[...] = jax.nn.gelu(proj.astype(BF16).astype(F32))
        if layer == 0:
            later(2, 3)
        with jax.named_scope("w_carry"):
            bytes_of(carries.at[layer, pl.ds(0, S - 1)], carry_sems.at[layer, 1]).wait()

        def fold(j, held):
            ahead, behind = held
            one = carries[layer, j]
            ahead = jnp.where(j < p, one[0:1] * ahead + one[1:2], ahead)
            k = S - 1 - j
            one = carries[layer, k]
            behind = jnp.where(k > p, one[0:1] * behind + one[1:2], behind)
            return ahead, behind

        zero = jnp.zeros((1, width), F32)
        enter = lax.fori_loop(0, S, fold, (zero, zero), unroll=True)
        heads = [a * e + h for (a, h), e in zip(first, enter)]
        for r in range(seg):
            both = (
                local[0, 1, r]
                + local[0, 0, r] * heads[0]
                + local[1, 1, r]
                + local[1, 0, r] * heads[1]
            )
            for lane in range(width // 128):
                hidden[lane, pl.ds(r, 8, stride=seg), :] = both[:, lane * 128 : (lane + 1) * 128]
        states = jnp.concatenate([hidden[lane] for lane in range(width // 128)], axis=1)
        mix = (gated[...] * states).astype(BF16)
        across = spread[2 * layer + 1]
        acts[2 * layer + 1, t] = mix
        across.begin()
        if layer == 0:
            later(4)
        with jax.named_scope("w_mix1"):
            across.step(1)
        if layer == 0:
            later(5, 6)
            with jax.named_scope("w_joinout"):
                ring_out.joined()
        with jax.named_scope("w_mix"):
            across.wait(2)
        full = acts.at[2 * layer + 1]
        moved = jnp.zeros((rows, width), F32)
        for k in range(T):
            moved = moved + jnp.dot(full[k], weight(out_at, k), preferred_element_type=F32)
        before = tokens[...] if layer == 0 else block[...]
        resid = (before.astype(F32) + moved).astype(BF16)
        if layer < LAYERS - 1:
            block[...] = resid
            acts[2, t] = resid
            spread[2].begin()
            later(7)
            with jax.named_scope("w_resid1"):
                spread[2].step(1)
            later(8)
            with jax.named_scope("w_joinc"):
                ring_c.joined()
            with jax.named_scope("w_resid"):
                spread[2].wait(2)
            normalize(1)

    wide = resid.astype(F32)
    own = jnp.sum(wide * wide, axis=1, keepdims=True)
    line = jnp.broadcast_to(own, (rows, rows)).T[0:1]
    squares[t] = line
    for d in range(1, T):
        copy = remote(
            squares.at[t], squares.at[t], square_sems.at[0], square_sems.at[1],
            {"tp": lax.rem(t + d, T)},
        )
        copy.start()
    with jax.named_scope("w_drain"):
        for each in (*rings, *spread):
            each.drain()
        for layer in range(LAYERS):
            bytes_of(carries.at[layer, pl.ds(0, S - 1)], carry_sems.at[layer, 0]).wait()
    with jax.named_scope("w_sq"):
        bytes_of(squares.at[pl.ds(0, T - 1)], square_sems.at[1]).wait()
    total = squares[0]
    for k in range(1, T):
        total = total + squares[k]
    scale = lax.rsqrt(total / (T * width) + EPS)
    scale = jnp.broadcast_to(scale, (rows, rows)).T[:, 0:1]
    out[...] = (wide * scale * final_gain[...]).astype(BF16)
    bytes_of(squares.at[pl.ds(0, T - 1)], square_sems.at[0]).wait()


def body(S, T, *args):
    tokens, gate_maps, in_weight = args[0], args[6], args[2]
    args = (*args[:6], jnp.swapaxes(gate_maps, 1, 2), args[7], args[8][None])
    rows, width = tokens.shape
    depth = in_weight.shape[1]
    cols = gate_maps.shape[2]
    seg = rows // 8
    dma = pltpu.SemaphoreType.DMA
    return pl.pallas_call(
        functools.partial(kernel, S, T),
        out_shape=jax.ShapeDtypeStruct((rows, width), BF16),
        in_specs=[pl.BlockSpec(memory_space=pltpu.HBM)] * len(args),
        out_specs=pl.BlockSpec(memory_space=pltpu.VMEM),
        scratch_shapes=[
            pltpu.VMEM((rows, width), BF16),
            pltpu.VMEM(args[1].shape, F32),
            pltpu.VMEM(args[4].shape, F32),
            pltpu.VMEM(args[5].shape, F32),
            pltpu.VMEM((1, width), F32),
            pltpu.VMEM((S, depth, width), BF16),
            pltpu.VMEM((S, cols, width), BF16),
            pltpu.VMEM((S, depth, width), BF16),
            pltpu.VMEM((S, depth, width), BF16),
            pltpu.VMEM((S, depth + cols, width), BF16),
            pltpu.VMEM((S, 2 * depth, width), BF16),
            pltpu.VMEM((4, T, rows, width), BF16),
            pltpu.VMEM((T, rows, width), BF16),
            pltpu.VMEM((LAYERS, 2, 16, width), BF16),
            pltpu.VMEM((LAYERS, 2, 16, width), BF16),
            pltpu.VMEM((rows + 16, width), F32),
            pltpu.VMEM((2, width // 128, rows, 128), F32),
            pltpu.VMEM((2, 2, seg, 8, width), F32),
            pltpu.VMEM((width // 128, rows, 128), F32),
            pltpu.VMEM((rows, width), F32),
            pltpu.VMEM((LAYERS, 2, 2, width), F32),
            pltpu.VMEM((LAYERS, S, 2, width), F32),
            pltpu.VMEM((rows, width), BF16),
            pltpu.VMEM((T, 1, rows), F32),
            dma((13,)),
            dma((6, 2, S // 4)),
            dma((6, 3)),
            dma((4, 2, T // 2)),
            dma((4,)),
            dma((LAYERS, 4)),
            dma((LAYERS, 2)),
            dma((2,)),
        ],
        compiler_params=pltpu.CompilerParams(
            collective_id=0, has_side_effects=True
        ),
        name="recurrent_layers",
    )(*args)


def solution(mesh):
    placed = (
        P(("grp", "sp"), "tp"),
        P(),
        P(None, "sp", "tp"),
        P(None, "sp", "tp"),
        P(None, None, "tp"),
        P(None, None, "tp"),
        P(None, "tp", "sp"),
        P(None, "sp", "tp"),
        P("tp"),
    )
    return jax.shard_map(
        functools.partial(body, mesh.shape["sp"], mesh.shape["tp"]),
        mesh=mesh,
        in_specs=placed,
        out_specs=P(("grp", "sp"), "tp"),
        check_vma=False,
    )
```

time: 173 us -> 144 us (0.83)
  Pallas kernels: 169 us -> 142 us
  local copies, waits for them, and re-layouts: 3.29 us -> 1.47 us
    pallas_call x1, Pallas kernels: 169 us -> 142 us  [body(): pl.pallas_call(functools.partial(kernel, S, T), out_shape=jax.ShapeDtypeS...]
    unnamed x18 -> x1, local copies, waits for them, and re-layouts: 3.29 us -> 1.47 us
where the time goes in v2:
time: 144 us
  Pallas kernels  142 us (99%)
  local copies, waits for them, and re-layouts  1.47 us (1%)
    pallas_call x1, Pallas kernels, body(): pl.pallas_call(functools.partial(kernel, S, T), out_shape=jax.ShapeDtypeS...  142 us

profile of v2, /device:TPU:80, one launch (start us, length us, event | category | flops | bytes accessed | tf_op | source)
XLA Modules:
  0.0 143.7 jit_solution(2530357653334185215)
XLA Ops:
  0.0 142.2 %recurrent_layers.1 = bf16[128,256]{1,0:T(8,128)(2,1)} custom-call(bf16[128,256]{1,0:T(8,128)(2,1)} %tokens_hbm.1, f32[2,2048]{1,0:T(2,128)} %norm_gain_hbm.1, bf16[2,64,256]{2,1,0:T(8,128)(2,1)} %in_weight.1, bf16[2,64,256]{2,1,0:T(8,128)(2,1)} %gate_weight.1, f32[2,4,256]{2,1,0:T(4,128)} %conv_taps_hbm.1, f32[2,2,256]{2,1,0:T(2,128)} %decay_logit_hbm.1, ...), custom_call_target="tpu_custom_call" | custom-call | tf_op jit(solution)/shard_map/recurrent_layers/pallas_call | solution.py:505
  142.2 1.5 %copy.11 = bf16[128,256]{1,0:T(8,128)(2,1)} copy(bf16[128,256]{1,0:T(8,128)(2,1)} %recurrent_layers.1) | data formatting | bytes 131072

commit v3 on v2

--- a/solution.py
+++ b/solution.py
@@ -55,7 +55,7 @@
             self.push_send, self.push_recv = sems[2:]
         self.rows = held.shape[1]
         self.stages = -(-self.half // reach)
-        self.last = self.stages
+        self.done = 0
 
     def slot(self, place):
         place = lax.rem(place + 2 * self.size, self.size)
@@ -115,6 +115,13 @@
         for stage in range(first, self.stages + 1):
             self.step(stage)
 
+    def advance(self):
+        if self.done == 0:
+            self.begin()
+        elif self.done <= self.stages:
+            self.step(self.done)
+        self.done += 1
+
     def joined(self):
         bytes_of(self.held.at[pl.ds(0, self.size)], self.push_recv).wait()
 
@@ -124,9 +131,12 @@
             bytes_of(self.held.at[pl.ds(0, self.size)], self.push_send).wait()
 
 
-REACH_IN = 1
-REACH_LATER = 1
+REACH = (2, 2, 2, 2, 2, 2, 2)
 REACH_X = 2
+PARTS = 2
+SLOTS = dict(
+    a1="m", a2="mg", a3="mg", a4="mgo", x0="g", k0="oc", y0="o", p0="oc", q0="cd", r0="cd", s0="de", x1="de", y1="e", p1="e"
+)
 
 
 def kernel(
@@ -142,7 +152,6 @@
     out_weight,
     final_gain_hbm,
     out,
-    tokens,
     norm_gain,
     conv_taps,
     decay_logit,
@@ -153,6 +162,7 @@
     held_out,
     held_c,
     held_d,
+    held_e,
     acts,
     normed,
     edges,
@@ -177,14 +187,14 @@
 ):
     p = lax.axis_index("sp")
     t = lax.axis_index("tp")
-    rows, width = tokens.shape
+    rows, width = acts.shape[2:]
     depth = in_weight.shape[1]
     cols = gate_maps.shape[1]
     seg = rows // 8
     share = width // depth
     quarter = S // 4
 
-    held = (held_in, held_map, held_gate, held_out, held_c, held_d)
+    held = (held_in, held_map, held_gate, held_out, held_c, held_d, held_e)
     rings = [
         Gather(
             g,
@@ -192,22 +202,49 @@
             "sp",
             S,
             p,
-            REACH_IN if k < 2 else REACH_LATER,
+            REACH[k],
             True,
         )
         for k, g in enumerate(held)
     ]
-    ring_in, ring_map, ring_gate, ring_out, ring_c, ring_d = rings
+    ring_in, ring_map, ring_gate, ring_out, ring_c, ring_d, ring_e = rings
+    part = rows // PARTS
     spread = [
-        Gather(acts.at[k], (x_send.at[k], x_recv.at[k]), "tp", T, t, REACH_X, False)
+        [
+            Gather(
+                acts.at[k, :, pl.ds(h * part, part)],
+                (x_send.at[k, h], x_recv.at[k, h]),
+                "tp",
+                T,
+                t,
+                REACH_X,
+                False,
+            )
+            for h in range(PARTS)
+        ]
         for k in range(4)
     ]
+
+    def advance(*some):
+        for each in some:
+            with jax.named_scope("w_%d.%d" % (rings.index(each), each.done)):
+                each.advance()
+
+    def slot(name):
+        for k in SLOTS.get(name, ""):
+            advance(rings["imgocde".index(k)])
+
+    def finish(each):
+        with jax.named_scope("w_%d.f" % rings.index(each)):
+            while each.done <= each.stages:
+                each.advance()
+            each.joined()
 
     barrier = pltpu.get_barrier_semaphore()
     friends = [
         {"sp": ring_in.slot(ring_in.place + way * j)}
         for way in (1, -1)
-        for j in range(1, REACH_IN + 1)
+        for j in range(1, min(REACH[0], ring_in.half) + 1)
     ]
     friends.append({"sp": ring_in.place * 2 + 1 - ring_in.core})
     friends.extend({"tp": lax.rem(t + d, T)} for d in range(1, T))
@@ -219,13 +256,13 @@
     loads = [
         (in_weight.at[0], held_in.at[p]),
         (gate_maps.at[0], held_map.at[p]),
-        (tokens_hbm, tokens),
+        (tokens_hbm, acts.at[0, t]),
         (gate_weight.at[0], held_gate.at[p]),
         (out_weight.at[0], held_out.at[p]),
         (in_weight.at[1], held_c.at[p, pl.ds(0, depth)]),
         (gate_maps.at[1], held_c.at[p, pl.ds(depth, cols)]),
-        (gate_weight.at[1], held_d.at[p, pl.ds(0, depth)]),
-        (out_weight.at[1], held_d.at[p, pl.ds(depth, depth)]),
+        (gate_weight.at[1], held_d.at[p]),
+        (out_weight.at[1], held_e.at[p]),
         (norm_gain_hbm, norm_gain),
         (conv_taps_hbm, conv_taps),
         (decay_logit_hbm, decay_logit),
@@ -236,64 +273,52 @@
     ]
     for load in loads:
         load.start()
-    for load in loads:
+    for load in loads[:3]:
         load.wait()
-    acts[0, t] = tokens[...]
     with jax.named_scope("w_barrier"):
         pl.semaphore_wait(barrier, len(friends))
-
     ring_in.begin()
-    ring_map.begin()
-    spread[0].begin()
-
-    def normalize(layer):
-        full = acts.at[2 * layer]
-        total = jnp.zeros((rows, 1), F32)
+    for each in spread[0]:
+        each.begin()
+    slot("a0")
+    for load in loads[3:]:
+        load.wait()
+
+    def normalize(layer, h):
+        piece = slice(h * part, (h + 1) * part)
+        total = jnp.zeros((part, 1), F32)
         for k in range(T):
-            wide = full[k].astype(F32)
+            wide = acts[2 * layer, k, piece].astype(F32)
             total = total + jnp.sum(wide * wide, axis=1, keepdims=True)
         scale = lax.rsqrt(total / (T * width) + EPS)
         for k in range(T):
-            wide = full[k].astype(F32)
-            normed[k] = (
+            wide = acts[2 * layer, k, piece].astype(F32)
+            normed[k, piece] = (
                 wide * scale * norm_gain[layer : layer + 1, k * width : (k + 1) * width]
             ).astype(BF16)
 
-    lagged = [ring_gate, ring_out]
-    for step in range(1, ring_in.last + 1):
+    for step in range(1, ring_in.stages + 1):
         with jax.named_scope("w_in%d" % step):
             ring_in.step(step)
-            ring_map.step(step)
-        with jax.named_scope("w_go%d" % step):
-            for each in lagged:
-                if step == 1:
-                    each.begin()
-                elif step <= each.last:
-                    each.step(step - 1)
         if step == 1:
             with jax.named_scope("w_tok1"):
-                spread[0].step(1)
-        if step == max(1, ring_in.last - 1):
+                for each in spread[0]:
+                    each.step(1)
+        slot("a%d" % step)
+        if step == max(1, ring_in.stages - 1):
             with jax.named_scope("w_tokens"):
-                spread[0].wait(2)
-            normalize(0)
+                for each in spread[0]:
+                    each.wait(2)
+            for h in range(PARTS):
+                normalize(0, h)
     with jax.named_scope("w_join"):
         ring_in.joined()
-
-    def later(*steps):
-        for step in steps:
-            with jax.named_scope("w_c%d" % step):
-                for each in (ring_c, ring_d):
-                    if step == 0:
-                        each.begin()
-                    elif step <= each.last:
-                        each.step(step)
 
     for layer in range(LAYERS):
         if layer == 0:
             in_at, map_at, gate_at, out_at = (held_in, 0), (held_map, 0), (held_gate, 0), (held_out, 0)
         else:
-            in_at, map_at, gate_at, out_at = (held_c, 0), (held_c, depth), (held_d, 0), (held_d, depth)
+            in_at, map_at, gate_at, out_at = (held_c, 0), (held_c, depth), (held_d, 0), (held_e, 0)
 
         def weight(at, k):
             ref, row = at
@@ -317,15 +342,14 @@
         down.start()
         padded[8 : 8 + rows] = xin.astype(F32)
         if layer == 0:
-            with jax.named_scope("w_golast"):
-                ring_map.joined()
-                for each in lagged:
-                    for step in range(min(ring_in.last, each.last), each.last + 1):
-                        each.step(step)
-            later(0)
+            slot("x0")
+        else:
+            slot("x1")
         with jax.named_scope("w_halo"):
             up.wait()
             down.wait()
+        if layer == 0:
+            finish(ring_map)
         before = edge_in[layer, 0].astype(F32)[8:16]
         after = edge_in[layer, 1].astype(F32)[0:8]
         padded[0:8] = jnp.where(p == 0, 0.0, before)
@@ -397,18 +421,19 @@
         lax.fori_loop(1, S, tell, 0)
         carries[layer, p] = msg[layer, 0]
         if layer == 0:
-            later(1)
-            with jax.named_scope("w_joingate"):
-                ring_gate.joined()
+            slot("k0")
+            finish(ring_gate)
         else:
-            with jax.named_scope("w_joind"):
-                ring_d.joined()
+            slot("k1")
+            finish(ring_d)
         proj = jnp.zeros((rows, width), F32)
         for k in range(T):
             proj = proj + jnp.dot(normed[k], weight(gate_at, k), preferred_element_type=F32)
         gated[...] = jax.nn.gelu(proj.astype(BF16).astype(F32))
         if layer == 0:
-            later(2, 3)
+            slot("y0")
+        else:
+            slot("y1")
         with jax.named_scope("w_carry"):
             bytes_of(carries.at[layer, pl.ds(0, S - 1)], carry_sems.at[layer, 1]).wait()
 
@@ -437,37 +462,45 @@
         mix = (gated[...] * states).astype(BF16)
         across = spread[2 * layer + 1]
         acts[2 * layer + 1, t] = mix
-        across.begin()
+        for each in across:
+            each.begin()
+        slot("p%d" % layer)
+        with jax.named_scope("w_mix1"):
+            for each in across:
+                each.step(1)
         if layer == 0:
-            later(4)
-        with jax.named_scope("w_mix1"):
-            across.step(1)
-        if layer == 0:
-            later(5, 6)
-            with jax.named_scope("w_joinout"):
-                ring_out.joined()
-        with jax.named_scope("w_mix"):
-            across.wait(2)
-        full = acts.at[2 * layer + 1]
-        moved = jnp.zeros((rows, width), F32)
-        for k in range(T):
-            moved = moved + jnp.dot(full[k], weight(out_at, k), preferred_element_type=F32)
-        before = tokens[...] if layer == 0 else block[...]
-        resid = (before.astype(F32) + moved).astype(BF16)
+            slot("q0")
+            finish(ring_out)
+        else:
+            finish(ring_e)
+        for h in range(PARTS):
+            with jax.named_scope("w_mix"):
+                across[h].wait(2)
+            piece = slice(h * part, (h + 1) * part)
+            moved = jnp.zeros((part, width), F32)
+            for k in range(T):
+                moved = moved + jnp.dot(
+                    acts[2 * layer + 1, k, piece], weight(out_at, k), preferred_element_type=F32
+                )
+            resid = (acts[2 * layer, t, piece].astype(F32) + moved).astype(BF16)
+            if layer < LAYERS - 1:
+                acts[2, t, piece] = resid
+                spread[2][h].begin()
+            else:
+                block[piece] = resid
         if layer < LAYERS - 1:
-            block[...] = resid
-            acts[2, t] = resid
-            spread[2].begin()
-            later(7)
+            slot("r0")
             with jax.named_scope("w_resid1"):
-                spread[2].step(1)
-            later(8)
-            with jax.named_scope("w_joinc"):
-                ring_c.joined()
-            with jax.named_scope("w_resid"):
-                spread[2].wait(2)
-            normalize(1)
-
+                for each in spread[2]:
+                    each.step(1)
+            slot("s0")
+            for h in range(PARTS):
+                with jax.named_scope("w_resid"):
+                    spread[2][h].wait(2)
+                normalize(1, h)
+            finish(ring_c)
+
+    resid = block[...]
     wide = resid.astype(F32)
     own = jnp.sum(wide * wide, axis=1, keepdims=True)
     line = jnp.broadcast_to(own, (rows, rows)).T[0:1]
@@ -479,7 +512,7 @@
         )
         copy.start()
     with jax.named_scope("w_drain"):
-        for each in (*rings, *spread):
+        for each in (*rings, *sum(spread, [])):
             each.drain()
         for layer in range(LAYERS):
             bytes_of(carries.at[layer, pl.ds(0, S - 1)], carry_sems.at[layer, 0]).wait()
@@ -508,7 +541,6 @@
         in_specs=[pl.BlockSpec(memory_space=pltpu.HBM)] * len(args),
         out_specs=pl.BlockSpec(memory_space=pltpu.VMEM),
         scratch_shapes=[
-            pltpu.VMEM((rows, width), BF16),
             pltpu.VMEM(args[1].shape, F32),
             pltpu.VMEM(args[4].shape, F32),
             pltpu.VMEM(args[5].shape, F32),
@@ -518,7 +550,8 @@
             pltpu.VMEM((S, depth, width), BF16),
             pltpu.VMEM((S, depth, width), BF16),
             pltpu.VMEM((S, depth + cols, width), BF16),
-            pltpu.VMEM((S, 2 * depth, width), BF16),
+            pltpu.VMEM((S, depth, width), BF16),
+            pltpu.VMEM((S, depth, width), BF16),
             pltpu.VMEM((4, T, rows, width), BF16),
             pltpu.VMEM((T, rows, width), BF16),
             pltpu.VMEM((LAYERS, 2, 16, width), BF16),
@@ -533,10 +566,10 @@
             pltpu.VMEM((rows, width), BF16),
             pltpu.VMEM((T, 1, rows), F32),
             dma((13,)),
-            dma((6, 2, S // 4)),
-            dma((6, 3)),
-            dma((4, 2, T // 2)),
-            dma((4,)),
+            dma((7, 2, S // 4)),
+            dma((7, 3)),
+            dma((4, PARTS, 2, T // 2)),
+            dma((4, PARTS)),
             dma((LAYERS, 4)),
             dma((LAYERS, 2)),
             dma((2,)),

time: 144 us -> 137 us (0.951)
  Pallas kernels: 142 us -> 136 us
    pallas_call x1, Pallas kernels: 142 us -> 136 us  [body(): pl.pallas_call(functools.partial(kernel, S, T), out_shape=jax.ShapeDtypeS...]
where the time goes in v3:
time: 137 us
  Pallas kernels  136 us (99%)
  local copies, waits for them, and re-layouts  1.47 us (1%)
    pallas_call x1, Pallas kernels, body(): pl.pallas_call(functools.partial(kernel, S, T), out_shape=jax.ShapeDtypeS...  136 us

profile of v3, /device:TPU:80, one launch (start us, length us, event | category | flops | bytes accessed | tf_op | source)
XLA Modules:
  0.0 137.1 jit_solution(4410787408817392088)
XLA Ops:
  0.0 135.6 %recurrent_layers.1 = bf16[128,256]{1,0:T(8,128)(2,1)} custom-call(bf16[128,256]{1,0:T(8,128)(2,1)} %tokens_hbm.1, f32[2,2048]{1,0:T(2,128)} %norm_gain_hbm.1, bf16[2,64,256]{2,1,0:T(8,128)(2,1)} %in_weight.1, bf16[2,64,256]{2,1,0:T(8,128)(2,1)} %gate_weight.1, f32[2,4,256]{2,1,0:T(4,128)} %conv_taps_hbm.1, f32[2,2,256]{2,1,0:T(2,128)} %decay_logit_hbm.1, ...), custom_call_target="tpu_custom_call" | custom-call | tf_op jit(solution)/shard_map/recurrent_layers/pallas_call | solution.py:538
  135.7 1.5 %copy.11 = bf16[128,256]{1,0:T(8,128)(2,1)} copy(bf16[128,256]{1,0:T(8,128)(2,1)} %recurrent_layers.1) | data formatting | bytes 131072

commit v4 on v3

--- a/solution.py
+++ b/solution.py
@@ -36,10 +36,10 @@
     return jnp.maximum(x, 0.0) + jnp.where(y < 0.05, series, jnp.log(1.0 + y))
 
 
-def neg_expm1(x):
+def neg_expm1(x, half):
     tail = 1 + x * (1 / 6) * (1 + x * (1 / 7) * (1 + x * (1 / 8)))
     series = x * (1 + x * (1 / 2) * (1 + x * (1 / 3) * (1 + x * (1 / 4) * (1 + x * (1 / 5) * tail))))
-    return -jnp.where(x > -0.5, series, jnp.exp(x) - 1.0)
+    return jnp.where(x > -0.5, -series, 1.0 - half * half)
 
 
 class Gather:
@@ -374,7 +374,7 @@
                 -8.0 * gate(2 * way) * softplus_small(-decay_logit[layer, way : way + 1])
             )
             decay = jnp.exp(log_a)
-            drive = jnp.sqrt(neg_expm1(2.0 * log_a)) * gate(2 * way + 1) * conv32
+            drive = jnp.sqrt(neg_expm1(2.0 * log_a, decay)) * gate(2 * way + 1) * conv32
             for lane in range(width // 128):
                 coef[0, lane] = decay[:, lane * 128 : (lane + 1) * 128]
                 coef[1, lane] = drive[:, lane * 128 : (lane + 1) * 128]
@@ -505,6 +505,7 @@
     own = jnp.sum(wide * wide, axis=1, keepdims=True)
     line = jnp.broadcast_to(own, (rows, rows)).T[0:1]
     squares[t] = line
+    weighed = wide * final_gain[...]
     for d in range(1, T):
         copy = remote(
             squares.at[t], squares.at[t], square_sems.at[0], square_sems.at[1],
@@ -523,7 +524,7 @@
         total = total + squares[k]
     scale = lax.rsqrt(total / (T * width) + EPS)
     scale = jnp.broadcast_to(scale, (rows, rows)).T[:, 0:1]
-    out[...] = (wide * scale * final_gain[...]).astype(BF16)
+    out[...] = (weighed * scale).astype(BF16)
     bytes_of(squares.at[pl.ds(0, T - 1)], square_sems.at[0]).wait()
 
 

time: 137 us -> 137 us (level)
  no operation moved by 1% of the time
where the time goes in v4:
time: 137 us
  Pallas kernels  136 us (99%)
  local copies, waits for them, and re-layouts  1.47 us (1%)
    pallas_call x1, Pallas kernels, body(): pl.pallas_call(functools.partial(kernel, S, T), out_shape=jax.ShapeDtypeS...  136 us

profile of v4, /device:TPU:80, one launch (start us, length us, event | category | flops | bytes accessed | tf_op | source)
XLA Modules:
  0.0 137.0 jit_solution(4461680402744429198)
XLA Ops:
  0.0 135.5 %recurrent_layers.1 = bf16[128,256]{1,0:T(8,128)(2,1)} custom-call(bf16[128,256]{1,0:T(8,128)(2,1)} %tokens_hbm.1, f32[2,2048]{1,0:T(2,128)} %norm_gain_hbm.1, bf16[2,64,256]{2,1,0:T(8,128)(2,1)} %in_weight.1, bf16[2,64,256]{2,1,0:T(8,128)(2,1)} %gate_weight.1, f32[2,4,256]{2,1,0:T(4,128)} %conv_taps_hbm.1, f32[2,2,256]{2,1,0:T(2,128)} %decay_logit_hbm.1, ...), custom_call_target="tpu_custom_call" | custom-call | tf_op jit(solution)/shard_map/recurrent_layers/pallas_call | solution.py:539
  135.5 1.5 %copy.11 = bf16[128,256]{1,0:T(8,128)(2,1)} copy(bf16[128,256]{1,0:T(8,128)(2,1)} %recurrent_layers.1) | data formatting | bytes 131072
